TPU v7x, 32 devices: a whole 2x2x4 slice. The times are simulated.
32 devices in a mesh: ep: 16 (over z, y, x), tp: 2 (over core).
Axes of the slice: x: 2, y: 2, z: 4, core: 2. Of those that a mesh axis runs over, the one named last changes fastest.
Arguments:
- inputs: bfloat16 [256, 2048], P('ep'), may hold values from -6 to 6
- positions: int32 [256], P('ep'), may hold values from 1024 to 8191
- ret_state: float32 [256, 12, 128, 128], P('ep', 'tp'), may hold values from -4 to 4
- norm_mix: bfloat16 [2048], replicated, may hold values from 0.099609375 to 1.8984375
- w_query: bfloat16 [2048, 1536], P('ep', 'tp'), may hold values from -0.1875 to 0.1875
- w_key: bfloat16 [2048, 1536], P('ep', 'tp'), may hold values from -0.1875 to 0.1875
- w_value: bfloat16 [2048, 1536], P('ep', 'tp'), may hold values from -0.1875 to 0.1875
- w_gate_in: bfloat16 [2048, 1536], P('ep', 'tp'), may hold values from -0.1875 to 0.1875
- head_gain: bfloat16 [1536], P('tp'), may hold values from 0.099609375 to 1.8984375
- w_out: bfloat16 [1536, 2048], P('tp', 'ep'), may hold values from -0.15625 to 0.15625
- norm_ffn: bfloat16 [2048], replicated, may hold values from 0.099609375 to 1.8984375
- route_ids: int32 [256, 4], P('ep'), may hold values from 0 to 15, all different within a row; in each aligned block of 16 rows (0 to 15, 16 to 31, ...) at most 8 rows name the same one
- route_weight: bfloat16 [256, 4], P('ep'), may hold values from 0.19921875 to 1
- exp_gate: bfloat16 [16, 2048, 1024], P('ep', None, 'tp'), may hold values from -0.125 to 0.125
- exp_up: bfloat16 [16, 2048, 1024], P('ep', None, 'tp'), may hold values from -0.125 to 0.125
- exp_down: bfloat16 [16, 1024, 2048], P('ep', 'tp'), may hold values from -0.1875 to 0.1875
- dense_gate: bfloat16 [2048, 4096], P(None, ('ep', 'tp')), may hold values from -0.125 to 0.125
- dense_up: bfloat16 [2048, 4096], P(None, ('ep', 'tp')), may hold values from -0.125 to 0.125
- dense_down: bfloat16 [4096, 2048], P(('ep', 'tp')), may hold values from -0.1875 to 0.1875
- branch_gate: bfloat16 [2048], replicated, may hold values from -0.125 to 0.125
Outputs:
- layer_out: bfloat16 [256, 2048], P('ep')
- new_state: float32 [256, 12, 128, 128], P('ep', 'tp')
Inputs may be any that keep to these rules, and one draw needn't show every extreme that they name: `route_ids`: each row names 4 different experts. Among the rows of one index of ep no expert is named more than 8 times, a bound that some block reaches.
All inputs are finite; a program needn't handle non-finite values.
Results may differ from a plain program's by a relative error of at most 0.015.
Values may be sent and summed in bfloat16 or wider, within the bound.
A program may use at most 128 MiB of HBM per device.

v0:
```python
import jax
import jax.numpy as jnp
from jax import lax
from jax.sharding import PartitionSpec as P

D = 2048
HEADS = 12
EPS = 1e-06


def rms_scale(values, scales):
    widened = values.astype(jnp.float32)
    scaled = widened * lax.rsqrt(jnp.mean(widened * widened, axis=-1, keepdims=True) + EPS)
    return (scaled * scales.astype(jnp.float32)).astype(jnp.bfloat16)


def rotary_angles(positions, head_dim):
    halfway = head_dim // 2
    frequency = 10000.0 ** (-jnp.arange(halfway, dtype=jnp.float32) * 2.0 / head_dim)
    return positions.astype(jnp.float32)[:, None] * frequency[None, :]


def rotate_heads(values, angles):
    halfway = values.shape[-1] // 2
    cosine = jnp.cos(angles)[:, None, :]
    sine_of = jnp.sin(angles)[:, None, :]
    leading = values[..., :halfway]
    trailing = values[..., halfway:]
    return jnp.concatenate(
        [leading * cosine - trailing * sine_of, trailing * cosine + leading * sine_of], axis=-1
    )


def log_decay(head_count):
    spread = jnp.arange(head_count, dtype=jnp.float32) * (5.0 / max(head_count - 1, 1))
    return jnp.log1p(-(2.0 ** (-5.0 - spread)))


def retain(queries, keys_in, values_in, gate_pre, old_state, positions, scales, log_gamma):
    row_count, head_count, head_dim = (old_state.shape[0], old_state.shape[1], old_state.shape[2])
    angles = rotary_angles(positions, head_dim)
    rot_query = rotate_heads(
        queries.astype(jnp.float32).reshape(row_count, head_count, head_dim), angles
    )
    rot_key = rotate_heads(
        keys_in.astype(jnp.float32).reshape(row_count, head_count, head_dim), angles
    ) * head_dim ** (-0.5)
    value_heads = values_in.astype(jnp.float32).reshape(row_count, head_count, head_dim)
    new_state = (
        jnp.exp(log_gamma)[None, :, None, None] * old_state
        + rot_key[:, :, :, None] * value_heads[:, :, None, :]
    )
    readout = jnp.einsum("shd,shdv->shv", rot_query, new_state, precision=lax.Precision.HIGHEST)
    centred = readout - jnp.mean(readout, axis=-1, keepdims=True)
    normed = centred * lax.rsqrt(jnp.mean(centred * centred, axis=-1, keepdims=True) + EPS)
    normed = normed * scales.astype(jnp.float32).reshape(head_count, head_dim)
    gated_out = normed.reshape(row_count, head_count * head_dim) * jax.nn.silu(
        gate_pre.astype(jnp.float32)
    )
    return (gated_out.astype(jnp.bfloat16), new_state)


def slot_of(route_ids, expert_count, capacity):
    flat_ids = route_ids.reshape(-1)
    onehot = (flat_ids[:, None] == jnp.arange(expert_count, dtype=jnp.int32)[None, :]).astype(
        jnp.int32
    )
    ranking = jnp.sum((jnp.cumsum(onehot, axis=0) - 1) * onehot, axis=1)
    return flat_ids * capacity + ranking


def on_device(
    inputs,
    positions,
    ret_state,
    norm_mix,
    w_query,
    w_key,
    w_value,
    w_gate_in,
    head_gain,
    w_out,
    norm_ffn,
    route_ids,
    route_weight,
    exp_gate,
    exp_up,
    exp_down,
    dense_gate,
    dense_up,
    dense_down,
    branch_gate,
):
    seq_count = inputs.shape[0]
    top_count = route_ids.shape[1]
    ep_size = lax.axis_size("ep")
    local_experts = exp_gate.shape[0]
    expert_count = ep_size * local_experts
    capacity = max(2, 2 * seq_count * top_count // expert_count)
    normed = rms_scale(inputs, norm_mix)
    columns = lax.all_to_all(normed, "ep", split_axis=1, concat_axis=0, tiled=True)
    joined = jnp.concatenate([w_query, w_key, w_value, w_gate_in], axis=1)
    segment = columns
    summed = lax.psum_scatter(
        jnp.dot(segment, joined, preferred_element_type=jnp.float32),
        "ep",
        scatter_dimension=0,
        tiled=True,
    ).astype(jnp.bfloat16)
    queries, keys_new, values_new, gate_pre = jnp.split(summed, 4, axis=1)
    local_heads = ret_state.shape[1]
    log_gamma = lax.dynamic_slice_in_dim(
        log_decay(HEADS), lax.axis_index("tp") * local_heads, local_heads
    )
    retained, new_state = retain(
        queries, keys_new, values_new, gate_pre, ret_state, positions, head_gain, log_gamma
    )
    partial_cols = jnp.dot(
        lax.all_gather(retained, "ep", axis=0, tiled=True),
        w_out,
        preferred_element_type=jnp.float32,
    )
    rounded = lax.optimization_barrier(partial_cols.astype(jnp.bfloat16)).astype(jnp.float32)
    mixer_cols = lax.psum(rounded.astype(jnp.bfloat16), "tp")
    mixer_out = lax.all_to_all(mixer_cols, "ep", split_axis=0, concat_axis=1, tiled=True)
    residual_sum = (inputs.astype(jnp.float32) + mixer_out.astype(jnp.float32)).astype(jnp.bfloat16)
    normed_ffn = rms_scale(residual_sum, norm_ffn)
    slot_index = slot_of(route_ids, expert_count, capacity)
    slot_total = expert_count * capacity
    placing = (jnp.arange(slot_total, dtype=jnp.int32)[:, None] == slot_index[None, :]).astype(
        jnp.float32
    )
    by_token = jnp.sum(placing.reshape(slot_total, seq_count, top_count), axis=2)
    outgoing = (
        jnp.dot(by_token.astype(jnp.bfloat16), normed_ffn, preferred_element_type=jnp.float32)
        .astype(jnp.bfloat16)
        .reshape(expert_count, capacity, D)
    )
    received = lax.all_to_all(outgoing, "ep", split_axis=0, concat_axis=0, tiled=True)
    slot_count = received.shape[1]
    grouped = received.reshape(ep_size, local_experts, slot_count, D)
    gate_part = jnp.einsum("sjnd,jdf->sjnf", grouped, exp_gate, preferred_element_type=jnp.float32)
    up_part = jnp.einsum("sjnd,jdf->sjnf", grouped, exp_up, preferred_element_type=jnp.float32)
    hidden = (jax.nn.silu(gate_part) * up_part).astype(jnp.bfloat16)
    partial_out = jnp.einsum(
        "sjnf,jfd->sjnd", hidden, exp_down, preferred_element_type=jnp.float32
    ).reshape(received.shape[0], slot_count, D)
    returned = lax.all_to_all(
        partial_out.astype(jnp.bfloat16), "ep", split_axis=0, concat_axis=0, tiled=True
    ).astype(partial_out.dtype)
    widened = route_weight.astype(jnp.float32)
    share_flat = (widened / jnp.sum(widened, axis=-1, keepdims=True)).reshape(-1)
    weighting = jnp.sum(
        (placing * share_flat[None, :]).reshape(slot_total, seq_count, top_count), axis=2
    )
    expert_part = jnp.einsum(
        "rt,rd->td", weighting, returned.reshape(slot_total, D), precision=lax.Precision.HIGHEST
    )
    segment = lax.all_gather(normed_ffn, "ep", axis=0, tiled=True)
    gate_part = jnp.dot(segment, dense_gate, preferred_element_type=jnp.float32)
    up_part = jnp.dot(segment, dense_up, preferred_element_type=jnp.float32)
    hidden = (jax.nn.silu(gate_part) * up_part).astype(jnp.bfloat16)
    opening = jax.nn.sigmoid(
        jnp.dot(segment, branch_gate[:, None], preferred_element_type=jnp.float32)
    )
    branch_term = jnp.dot(hidden, dense_down, preferred_element_type=jnp.float32) * opening
    summed_branch = lax.psum_scatter(branch_term, "ep", scatter_dimension=0, tiled=True)
    summed_branch = summed_branch + expert_part
    width_total = lax.psum(summed_branch.astype(jnp.bfloat16), "tp").astype(jnp.float32)
    layer_out = (residual_sum.astype(jnp.float32) + width_total).astype(jnp.bfloat16)
    return (layer_out, new_state)


def solution(mesh):
    in_specs = (
        P("ep", None),
        P("ep"),
        P("ep", "tp", None, None),
        P(),
        P("ep", "tp"),
        P("ep", "tp"),
        P("ep", "tp"),
        P("ep", "tp"),
        P("tp"),
        P("tp", "ep"),
        P(),
        P("ep", None),
        P("ep", None),
        P("ep", None, "tp"),
        P("ep", None, "tp"),
        P("ep", "tp", None),
        P(None, ("ep", "tp")),
        P(None, ("ep", "tp")),
        P(("ep", "tp"), None),
        P(),
    )
    out_specs = (P("ep", None), P("ep", "tp", None, None))
    return jax.shard_map(
        on_device, mesh=mesh, in_specs=in_specs, out_specs=out_specs, check_vma=False
    )
```

profile of v0, /device:TPU:0, one launch (start us, length us, event | category | flops | bytes accessed | tf_op | source)
XLA Modules:
  0.0 408.9 jit_solution(14892159099410248619)
XLA Ops:
  7.2 0.8 convert_element_type.89
  8.1 1.0 fusion.39
  9.0 0.9 copy_bitcast_fusion
  10.0 15.7 %all_to_all.42 = bf16[16,16,128]{2,0,1:T(8,128)(2,1)S(1)} all-to-all(bf16[16,16,128]{2,0,1:T(8,128)(2,1)S(1)} %copy_bitcast_fusion), channel_id=1, replica_groups=mesh['ep'=16,'tp'=2] {'ep'}, dimensions={1} | all-to-all | bytes 131072 | tf_op jit(solution)/shard_map/all_to_all | solution.py:101
  25.6 3.4 fusion.25
  29.2 0.6 copy-done.11
  30.0 128.4 %reduce-scatter.3.cloned.1.call-done = f32[16,3072]{1,0:T(8,128)} async-done(((f32[256,3072]{1,0:T(8,128)}), f32[16,3072]{1,0:T(8,128)}) %reduce-scatter.3.cloned.1.call-update) | async-done | bytes 196624 | tf_op jit(solution)/shard_map/reduce_scatter | solution.py:104
  158.3 0.9 convert_element_type.91
  159.7 4.5 %multiply_add_fusion = f32[16,6,128,128]{3,2,1,0:T(8,128)S(1)} fusion(f32[16,6,128,128]{3,2,1,0:T(8,128)} %param.22, f32[16,6,128]{2,1,0:T(8,128)S(1)} %reshape.211, f32[16,6,128]{2,1,0:T(8,128)S(1)} %maximum_multiply_fusion, f32[6]{0:T(128)S(1)} %dynamic-slice_exponential_fusion), kind=kLoop, calls=%fused_computation | loop fusion | flops 4718592 | bytes 12681240 | tf_op jit(solution)/shard_map/add | solution.py:50
  164.2 5.5 %fusion.63 = f32[16,6,1,128]{3,2,1,0:T(1,128)S(1)} fusion(f32[16,6,128,128]{3,2,1,0:T(8,128)S(1)} %multiply_add_fusion, f32[16,6,128,1]{2,1,0,3:T(8,128)S(1)} %maximum_bitcast_fusion), kind=kOutput, calls=%fused_computation.76 | convolution fusion | flops 18874368 | bytes 6389760 | tf_op jit(solution)/shard_map/shd,shdv->shv/dot_general | solution.py:53
  169.7 0.2 fusion.56
  170.1 40.8 %all_gather.6 = bf16[256,768]{1,0:T(8,128)(2,1)S(1)} all-gather(bf16[16,768]{1,0:T(8,128)(2,1)S(1)} %fusion.65), channel_id=1, replica_groups=mesh['ep'=16,'tp'=2] {'ep'}, dimensions={0}, use_global_device_ids=true | all-gather | bytes 417792 | tf_op jit(solution)/shard_map/all_gather | solution.py:119
  210.9 0.9 convolution_convert_fusion.2
  211.8 13.7 %all-reduce.3.cloned.1.call-done = bf16[16,16,128]{2,1,0:T(8,128)(2,1)} async-done(((bf16[16,16,128]{2,1,0:T(8,128)(2,1)}), bf16[16,16,128]{2,1,0:T(8,128)(2,1)}) %all-reduce.3.cloned.1.call-update) | async-done | bytes 65552 | tf_op jit(solution)/shard_map/psum | solution.py:124
  225.5 6.8 %all-to-all-start.1 = ((bf16[16,16,128]{2,1,0:T(8,128)(2,1)}), bf16[16,16,128]{2,1,0:T(8,128)(2,1)S(1)}, u32[]{:S(2)}, u32[]{:S(2)}) async-start(bf16[16,16,128]{2,1,0:T(8,128)(2,1)} %all-reduce.3.cloned.1.call-done), calls=%async_computation.2 | async-start | bytes 131072 | tf_op jit(solution)/shard_map/all_to_all | solution.py:125
  232.4 7.5 %all-to-all-done.1 = bf16[16,16,128]{2,1,0:T(8,128)(2,1)S(1)} async-done(((bf16[16,16,128]{2,1,0:T(8,128)(2,1)}), bf16[16,16,128]{2,1,0:T(8,128)(2,1)S(1)}, u32[]{:S(2)}, u32[]{:S(2)}) %all-to-all-start.1) | async-done | bytes 65568 | tf_op jit(solution)/shard_map/all_to_all | solution.py:125
  240.0 0.7 fusion.45
  240.9 52.0 %all-gather.2.cloned.1.call-done = bf16[256,2048]{1,0:T(8,128)(2,1)} async-done(((bf16[16,2048]{1,0:T(8,128)(2,1)}), bf16[256,2048]{1,0:T(8,128)(2,1)}) %all-gather.2.cloned.1.call-update) | async-done | bytes 1048592 | tf_op jit(solution)/shard_map/all_gather | solution.py:159
  292.9 1.7 fusion.73
  294.6 1.8 fusion.72
  296.4 3.3 convolution_multiply_fusion
  299.8 0.6 copy-done.6
  300.8 0.2 select_reduce_fusion.1
  301.3 0.3 fusion
  301.6 21.7 %all_to_all.43 = bf16[16,8,2048]{2,1,0:T(8,128)(2,1)S(1)} all-to-all(bf16[16,8,2048]{2,1,0:T(8,128)(2,1)S(1)} %fusion), channel_id=1, replica_groups=mesh['ep'=16,'tp'=2] {'ep'}, dimensions={0} | all-to-all | bytes 1048576 | tf_op jit(solution)/shard_map/all_to_all | solution.py:139
  323.3 2.0 fusion.7
  325.3 2.4 convolution_convert_fusion
  327.8 21.4 %all_to_all.44 = bf16[16,8,2048]{2,1,0:T(8,128)(2,1)S(1)} all-to-all(bf16[16,8,2048]{2,1,0:T(8,128)(2,1)S(1)} %convolution_convert_fusion), channel_id=1, replica_groups=mesh['ep'=16,'tp'=2] {'ep'}, dimensions={0} | all-to-all | bytes 1048576 | tf_op jit(solution)/shard_map/all_to_all | solution.py:148
  349.2 33.9 %reduce-scatter.5.cloned.1.call-done = f32[16,2048]{1,0:T(8,128)} async-done(((f32[256,2048]{1,0:T(8,128)}), f32[16,2048]{1,0:T(8,128)}) %reduce-scatter.5.cloned.1.call-update) | async-done | bytes 131088 | tf_op jit(solution)/shard_map/reduce_scatter | solution.py:167
  383.1 1.9 fusion.1
  385.0 15.9 %all-reduce.5.cloned.1.call-done = bf16[16,2048]{1,0:T(8,128)(2,1)} async-done(((bf16[16,2048]{1,0:T(8,128)(2,1)}), bf16[16,2048]{1,0:T(8,128)(2,1)}) %all-reduce.5.cloned.1.call-update) | async-done | bytes 65552 | tf_op jit(solution)/shard_map/psum | solution.py:169
  400.9 1.5 fusion.46
  (66 shorter events, 1.9 us)
Async XLA Ops:
  7.2 318.2 %copy-start = (bf16[1,512,2048]{2,1,0:T(8,128)(2,1)S(1)}, bf16[1,512,2048]{2,1,0:T(8,128)(2,1)}, u32[]{:S(2)}) copy-start(bf16[1,512,2048]{2,1,0:T(8,128)(2,1)} %param.35) | copy-start | bytes 6291460
  7.2 151.2 %reduce-scatter.3.cloned.1.call-start = ((), (), s32[]{:S(2)}) async-start(), calls=%async_computation.6 | async-start | bytes 3342336 | tf_op jit(solution)/shard_map/reduce_scatter | solution.py:104
  29.1 0.7 copy-start.11
  29.1 0.8 copy-start.9
  29.1 196.4 %all-reduce.3.cloned.1.call-start = ((), (), s32[]{:S(2)}) async-start(), calls=%async_computation.7 | async-start | bytes 131072 | tf_op jit(solution)/shard_map/psum | solution.py:124
  164.1 5.5 %copy-start.1 = (f32[16,6,128,128]{3,2,1,0:T(8,128)}, f32[16,6,128,128]{3,2,1,0:T(8,128)S(1)}, u32[]{:S(2)}) copy-start(f32[16,6,128,128]{3,2,1,0:T(8,128)S(1)} %multiply_add_fusion) | copy-start | bytes 18874372
  164.1 46.7 %copy-start.5 = (bf16[768,128]{1,0:T(8,128)(2,1)S(1)}, bf16[768,128]{1,0:T(8,128)(2,1)}, u32[]{:S(2)}) copy-start(bf16[768,128]{1,0:T(8,128)(2,1)} %param.29) | copy-start | bytes 589828
  164.1 68.3 %copy-start.7 = (bf16[2048]{0:T(1024)(128)(2,1)S(1)}, bf16[2048]{0:T(1024)(128)(2,1)}, u32[]{:S(2)}) copy-start(bf16[2048]{0:T(1024)(128)(2,1)} %param.30) | copy-start | bytes 12292
  164.2 75.7 %copy-start.3 = (bf16[16,2048]{1,0:T(8,128)(2,1)S(1)}, bf16[16,2048]{1,0:T(8,128)(2,1)}, u32[]{:S(2)}) copy-start(bf16[16,2048]{1,0:T(8,128)(2,1)} %param.20) | copy-start | bytes 196612
  169.6 71.2 %copy-start.8 = (bf16[2048]{0:T(1024)(128)(2,1)S(1)}, bf16[2048]{0:T(1024)(128)(2,1)}, u32[]{:S(2)}) copy-start(bf16[2048]{0:T(1024)(128)(2,1)} %param.39) | copy-start | bytes 12292
  225.5 14.4 %all-to-all-start.1 = ((bf16[16,16,128]{2,1,0:T(8,128)(2,1)}), bf16[16,16,128]{2,1,0:T(8,128)(2,1)S(1)}, u32[]{:S(2)}, u32[]{:S(2)}) async-start(bf16[16,16,128]{2,1,0:T(8,128)(2,1)} %all-reduce.3.cloned.1.call-done), calls=%async_computation.2 | async-start | bytes 131072 | tf_op jit(solution)/shard_map/all_to_all | solution.py:125
  232.4 60.6 %all-gather.2.cloned.1.call-start = ((), (), s32[]{:S(2)}) async-start(), calls=%async_computation.8 | async-start | bytes 1114112 | tf_op jit(solution)/shard_map/all_gather | solution.py:159
  240.8 142.3 %reduce-scatter.5.cloned.1.call-start = ((), (), s32[]{:S(2)}) async-start(), calls=%async_computation.9 | async-start | bytes 2228224 | tf_op jit(solution)/shard_map/reduce_scatter | solution.py:167
  292.9 3.5 copy-start.2
  299.8 0.7 copy-start.6
  299.8 1.4 copy-start.10
  299.8 1.5 copy-start.4
  299.8 101.1 %all-reduce.5.cloned.1.call-start = ((), (), s32[]{:S(2)}) async-start(), calls=%async_computation.10 | async-start | bytes 131072 | tf_op jit(solution)/shard_map/psum | solution.py:169
Sparse Core Ops, SparseCore 0:
  29.2 129.0 reduce-scatter.2
  211.9 13.5 all-reduce.2
  240.9 51.9 all-gather.1
  299.9 83.1 reduce-scatter.4
  385.8 15.0 all-reduce.4
where the time goes:
time: 410 us; the launch traced here: 409 us
  waiting for transfers between devices  251 us (61%)
  blocking collectives  99.6 us (24%)
  matrix products  23.2 us (6%)
  between operations  14.1 us (3%)
  other arithmetic  11.8 us (3%)
  starting transfers between devices  7.03 us (2%)
    reduce_scatter x1, waiting for transfers between devices, on_device(): lax.psum_scatter(jnp.dot(segment, joined, preferred_element_type=jnp.floa...  128 us
    all_gather x1, waiting for transfers between devices, on_device(): segment = lax.all_gather(normed_ffn, 'ep', axis=0, tiled=True)  52 us
    all_gather x1, blocking collectives, on_device(): lax.all_gather(retained, 'ep', axis=0, tiled=True)  40.8 us
    reduce_scatter x1, waiting for transfers between devices, on_device(): lax.psum_scatter(branch_term, 'ep', scatter_dimension=0, tiled=True)  33.9 us
    all_to_all x1, blocking collectives, on_device(): lax.all_to_all(outgoing, 'ep', split_axis=0, concat_axis=0, tiled=True)  21.7 us
    all_to_all x1, blocking collectives, on_device(): lax.all_to_all(partial_out.astype(jnp.bfloat16), 'ep', split_axis=0, conc...  21.4 us
    psum x1, waiting for transfers between devices, on_device(): lax.psum(summed_branch.astype(jnp.bfloat16), 'tp').astype(jnp.float32)  15.9 us
    all_to_all x1, blocking collectives, on_device(): lax.all_to_all(normed, 'ep', split_axis=1, concat_axis=0, tiled=True)  15.7 us
  transfers between devices with their start and end apart: 6, of which 6 were waited for; matrix products, arithmetic and copies ran while one was open for 1% of the time, Pallas kernels for 0%

commit v1 on v0

--- a/solution.py
+++ b/solution.py
@@ -116,7 +116,9 @@
         queries, keys_new, values_new, gate_pre, ret_state, positions, head_gain, log_gamma
     )
     partial_cols = jnp.dot(
-        lax.all_gather(retained, "ep", axis=0, tiled=True),
+        jnp.concatenate(
+            lax.all_to_all(jnp.stack([retained] * lax.axis_size("ep")), "ep", 0, 0), axis=0
+        ),
         w_out,
         preferred_element_type=jnp.float32,
     )

time: 410 us -> 387 us (0.944)
  blocking collectives: 99.6 us -> 74.4 us
    all_gather x1 -> x0, blocking collectives: 40.8 us -> none  [on_device(): lax.all_gather(retained, 'ep', axis=0, tiled=True)]
    all_to_all x0 -> x1, blocking collectives: none -> 15.6 us  [on_device(): lax.all_to_all(jnp.stack([retained] * lax.axis_size('ep')), 'ep', 0, 0)]
  transfers between devices with their start and end apart: 6 -> 6, of which waited for: 6 -> 6; matrix products, arithmetic and copies ran while one was open for 1% -> 2% of each run, Pallas kernels for 0% -> 0%
where the time goes in v1:
time: 387 us; the launch traced here: 386 us
  waiting for transfers between devices  254 us (66%)
  blocking collectives  74.4 us (19%)
  matrix products  23.2 us (6%)
  between operations  14.1 us (4%)
  other arithmetic  11.8 us (3%)
  starting transfers between devices  7.03 us (2%)
    reduce_scatter x1, waiting for transfers between devices, on_device(): lax.psum_scatter(jnp.dot(segment, joined, preferred_element_type=jnp.floa...  128 us
    all_gather x1, waiting for transfers between devices, on_device(): segment = lax.all_gather(normed_ffn, 'ep', axis=0, tiled=True)  52 us
    reduce_scatter x1, waiting for transfers between devices, on_device(): lax.psum_scatter(branch_term, 'ep', scatter_dimension=0, tiled=True)  33.8 us
    all_to_all x1, blocking collectives, on_device(): lax.all_to_all(outgoing, 'ep', split_axis=0, concat_axis=0, tiled=True)  21.7 us
    all_to_all x1, blocking collectives, on_device(): lax.all_to_all(partial_out.astype(jnp.bfloat16), 'ep', split_axis=0, conc...  21.5 us
    psum x1, waiting for transfers between devices, on_device(): lax.psum(summed_branch.astype(jnp.bfloat16), 'tp').astype(jnp.float32)  16.5 us
    psum x1, waiting for transfers between devices, on_device(): mixer_cols = lax.psum(rounded.astype(jnp.bfloat16), 'tp')  15.9 us
    all_to_all x1, blocking collectives, on_device(): lax.all_to_all(normed, 'ep', split_axis=1, concat_axis=0, tiled=True)  15.7 us
  transfers between devices with their start and end apart: 6, of which 6 were waited for; matrix products, arithmetic and copies ran while one was open for 2% of the time, Pallas kernels for 0%

profile of v1, /device:TPU:0, one launch (start us, length us, event | category | flops | bytes accessed | tf_op | source)
XLA Modules:
  0.0 386.4 jit_solution(11307829802066298847)
XLA Ops:
  7.2 0.8 convert_element_type.89
  8.1 1.0 fusion.39
  9.0 0.9 copy_bitcast_fusion
  10.0 15.7 %all_to_all.47 = bf16[16,16,128]{2,0,1:T(8,128)(2,1)S(1)} all-to-all(bf16[16,16,128]{2,0,1:T(8,128)(2,1)S(1)} %copy_bitcast_fusion), channel_id=1, replica_groups=mesh['ep'=16,'tp'=2] {'ep'}, dimensions={1} | all-to-all | bytes 131072 | tf_op jit(solution)/shard_map/all_to_all | solution.py:101
  25.6 3.4 fusion.25
  29.2 0.6 copy-done.11
  30.0 128.4 %reduce-scatter.3.cloned.1.call-done = f32[16,3072]{1,0:T(8,128)} async-done(((f32[256,3072]{1,0:T(8,128)}), f32[16,3072]{1,0:T(8,128)}) %reduce-scatter.3.cloned.1.call-update) | async-done | bytes 196624 | tf_op jit(solution)/shard_map/reduce_scatter | solution.py:104
  158.3 0.9 convert_element_type.91
  159.7 4.5 %multiply_add_fusion = f32[16,6,128,128]{3,2,1,0:T(8,128)S(1)} fusion(f32[16,6,128,128]{3,2,1,0:T(8,128)} %param.22, f32[16,6,128]{2,1,0:T(8,128)S(1)} %reshape.217, f32[16,6,128]{2,1,0:T(8,128)S(1)} %maximum_multiply_fusion, f32[6]{0:T(128)S(1)} %dynamic-slice_exponential_fusion), kind=kLoop, calls=%fused_computation | loop fusion | flops 4718592 | bytes 12681240 | tf_op jit(solution)/shard_map/add | solution.py:50
  164.1 5.5 %fusion.63 = f32[16,6,1,128]{3,2,1,0:T(1,128)S(1)} fusion(f32[16,6,128,128]{3,2,1,0:T(8,128)S(1)} %multiply_add_fusion, f32[16,6,128,1]{2,1,0,3:T(8,128)S(1)} %maximum_bitcast_fusion), kind=kOutput, calls=%fused_computation.76 | convolution fusion | flops 18874368 | bytes 6389760 | tf_op jit(solution)/shard_map/shd,shdv->shv/dot_general | solution.py:53
  169.7 0.2 fusion.56
  170.1 15.6 %all_to_all.48 = bf16[16,16,768]{2,1,0:T(8,128)(2,1)S(1)} all-to-all(bf16[16,16,768]{2,1,0:T(8,128)(2,1)S(1)} %stack.2), channel_id=1, replica_groups=mesh['ep'=16,'tp'=2] {'ep'}, dimensions={0} | all-to-all | bytes 786432 | tf_op jit(solution)/shard_map/all_to_all | solution.py:120
  185.7 0.9 convolution_convert_fusion.2
  186.6 15.9 %all-reduce.3.cloned.1.call-done = bf16[16,16,128]{2,1,0:T(8,128)(2,1)} async-done(((bf16[16,16,128]{2,1,0:T(8,128)(2,1)}), bf16[16,16,128]{2,1,0:T(8,128)(2,1)}) %all-reduce.3.cloned.1.call-update) | async-done | bytes 65552 | tf_op jit(solution)/shard_map/psum | solution.py:126
  202.5 6.8 %all-to-all-start.2 = ((bf16[16,16,128]{2,1,0:T(8,128)(2,1)}), bf16[16,16,128]{2,1,0:T(8,128)(2,1)S(1)}, u32[]{:S(2)}, u32[]{:S(2)}) async-start(bf16[16,16,128]{2,1,0:T(8,128)(2,1)} %all-reduce.3.cloned.1.call-done), calls=%async_computation.3 | async-start | bytes 131072 | tf_op jit(solution)/shard_map/all_to_all | solution.py:127
  209.4 7.5 %all-to-all-done.2 = bf16[16,16,128]{2,1,0:T(8,128)(2,1)S(1)} async-done(((bf16[16,16,128]{2,1,0:T(8,128)(2,1)}), bf16[16,16,128]{2,1,0:T(8,128)(2,1)S(1)}, u32[]{:S(2)}, u32[]{:S(2)}) %all-to-all-start.2) | async-done | bytes 65568 | tf_op jit(solution)/shard_map/all_to_all | solution.py:127
  217.0 0.7 fusion.45
  217.9 52.0 %all-gather.2.cloned.1.call-done = bf16[256,2048]{1,0:T(8,128)(2,1)} async-done(((bf16[16,2048]{1,0:T(8,128)(2,1)}), bf16[256,2048]{1,0:T(8,128)(2,1)}) %all-gather.2.cloned.1.call-update) | async-done | bytes 1048592 | tf_op jit(solution)/shard_map/all_gather | solution.py:161
  269.9 1.7 fusion.73
  271.6 1.8 fusion.72
  273.4 3.3 convolution_multiply_fusion
  276.8 0.6 copy-done.6
  277.8 0.2 select_reduce_fusion.1
  278.3 0.3 fusion
  278.6 21.7 %all_to_all.49 = bf16[16,8,2048]{2,1,0:T(8,128)(2,1)S(1)} all-to-all(bf16[16,8,2048]{2,1,0:T(8,128)(2,1)S(1)} %fusion), channel_id=1, replica_groups=mesh['ep'=16,'tp'=2] {'ep'}, dimensions={0} | all-to-all | bytes 1048576 | tf_op jit(solution)/shard_map/all_to_all | solution.py:141
  300.3 2.0 fusion.7
  302.3 2.4 convolution_convert_fusion
  304.8 21.5 %all_to_all.50 = bf16[16,8,2048]{2,1,0:T(8,128)(2,1)S(1)} all-to-all(bf16[16,8,2048]{2,1,0:T(8,128)(2,1)S(1)} %convolution_convert_fusion), channel_id=1, replica_groups=mesh['ep'=16,'tp'=2] {'ep'}, dimensions={0} | all-to-all | bytes 1048576 | tf_op jit(solution)/shard_map/all_to_all | solution.py:150
  326.2 33.8 %reduce-scatter.5.cloned.1.call-done = f32[16,2048]{1,0:T(8,128)} async-done(((f32[256,2048]{1,0:T(8,128)}), f32[16,2048]{1,0:T(8,128)}) %reduce-scatter.5.cloned.1.call-update) | async-done | bytes 131088 | tf_op jit(solution)/shard_map/reduce_scatter | solution.py:169
  360.0 1.9 fusion.1
  361.9 16.5 %all-reduce.5.cloned.1.call-done = bf16[16,2048]{1,0:T(8,128)(2,1)} async-done(((bf16[16,2048]{1,0:T(8,128)(2,1)}), bf16[16,2048]{1,0:T(8,128)(2,1)}) %all-reduce.5.cloned.1.call-update) | async-done | bytes 65552 | tf_op jit(solution)/shard_map/psum | solution.py:171
  378.4 1.5 fusion.46
  (67 shorter events, 2.0 us)
Async XLA Ops:
  7.2 295.2 %copy-start = (bf16[1,512,2048]{2,1,0:T(8,128)(2,1)S(1)}, bf16[1,512,2048]{2,1,0:T(8,128)(2,1)}, u32[]{:S(2)}) copy-start(bf16[1,512,2048]{2,1,0:T(8,128)(2,1)} %param.35) | copy-start | bytes 6291460
  7.2 151.2 %reduce-scatter.3.cloned.1.call-start = ((), (), s32[]{:S(2)}) async-start(), calls=%async_computation.7 | async-start | bytes 3342336 | tf_op jit(solution)/shard_map/reduce_scatter | solution.py:104
  29.1 0.7 copy-start.11
  29.1 0.8 copy-start.9
  29.1 173.4 %all-reduce.3.cloned.1.call-start = ((), (), s32[]{:S(2)}) async-start(), calls=%async_computation.8 | async-start | bytes 131072 | tf_op jit(solution)/shard_map/psum | solution.py:126
  164.1 5.5 %copy-start.1 = (f32[16,6,128,128]{3,2,1,0:T(8,128)}, f32[16,6,128,128]{3,2,1,0:T(8,128)S(1)}, u32[]{:S(2)}) copy-start(f32[16,6,128,128]{3,2,1,0:T(8,128)S(1)} %multiply_add_fusion) | copy-start | bytes 18874372
  164.1 21.6 %copy-start.5 = (bf16[768,128]{1,0:T(8,128)(2,1)S(1)}, bf16[768,128]{1,0:T(8,128)(2,1)}, u32[]{:S(2)}) copy-start(bf16[768,128]{1,0:T(8,128)(2,1)} %param.29) | copy-start | bytes 589828
  169.6 39.8 %copy-start.7 = (bf16[2048]{0:T(1024)(128)(2,1)S(1)}, bf16[2048]{0:T(1024)(128)(2,1)}, u32[]{:S(2)}) copy-start(bf16[2048]{0:T(1024)(128)(2,1)} %param.30) | copy-start | bytes 12292
  169.6 47.3 %copy-start.3 = (bf16[16,2048]{1,0:T(8,128)(2,1)S(1)}, bf16[16,2048]{1,0:T(8,128)(2,1)}, u32[]{:S(2)}) copy-start(bf16[16,2048]{1,0:T(8,128)(2,1)} %param.20) | copy-start | bytes 196612
  169.6 48.2 %copy-start.8 = (bf16[2048]{0:T(1024)(128)(2,1)S(1)}, bf16[2048]{0:T(1024)(128)(2,1)}, u32[]{:S(2)}) copy-start(bf16[2048]{0:T(1024)(128)(2,1)} %param.39) | copy-start | bytes 12292
  202.5 14.4 %all-to-all-start.2 = ((bf16[16,16,128]{2,1,0:T(8,128)(2,1)}), bf16[16,16,128]{2,1,0:T(8,128)(2,1)S(1)}, u32[]{:S(2)}, u32[]{:S(2)}) async-start(bf16[16,16,128]{2,1,0:T(8,128)(2,1)} %all-reduce.3.cloned.1.call-done), calls=%async_computation.3 | async-start | bytes 131072 | tf_op jit(solution)/shard_map/all_to_all | solution.py:127
  209.4 60.6 %all-gather.2.cloned.1.call-start = ((), (), s32[]{:S(2)}) async-start(), calls=%async_computation.9 | async-start | bytes 1114112 | tf_op jit(solution)/shard_map/all_gather | solution.py:161
  217.8 142.2 %reduce-scatter.5.cloned.1.call-start = ((), (), s32[]{:S(2)}) async-start(), calls=%async_computation.10 | async-start | bytes 2228224 | tf_op jit(solution)/shard_map/reduce_scatter | solution.py:169
  269.9 3.5 copy-start.2
  276.8 0.7 copy-start.6
  276.8 1.4 copy-start.10
  276.8 1.5 copy-start.4
  276.8 101.6 %all-reduce.5.cloned.1.call-start = ((), (), s32[]{:S(2)}) async-start(), calls=%async_computation.11 | async-start | bytes 131072 | tf_op jit(solution)/shard_map/psum | solution.py:171
Sparse Core Ops, SparseCore 0:
  29.2 129.0 reduce-scatter.2
  186.7 15.7 all-reduce.2
  217.9 51.9 all-gather.1
  276.9 83.0 reduce-scatter.4
  362.7 15.6 all-reduce.4
